TPU v7x, 32 devices: a whole 2x2x4 slice. The times are simulated.
32 devices in a mesh: fs: 8 (over z, y), tp: 4 (over x, core).
Axes of the slice: x: 2, y: 2, z: 4, core: 2. Of those that a mesh axis runs over, the one named last changes fastest.
Arguments:
- tokens: bfloat16 [3072, 2048], P('fs'), may hold values from -6 to 6
- first_norm_scale: float32 [2048], replicated, may hold values from 0.1 to 1.9
- recurrent_branch_matrix: bfloat16 [2048, 1024], P('fs', 'tp'), may hold values from -0.125 to 0.125
- gelu_gate_matrix: bfloat16 [2048, 1024], P('fs', 'tp'), may hold values from -0.125 to 0.125
- filter_taps_weight: bfloat16 [4, 1024], P(None, 'tp'), may hold values from -3 to 3
- recurrence_gate_blocks: bfloat16 [16, 64, 64], P('tp'), may hold values from -0.75 to 0.75
- input_gate_blocks: bfloat16 [16, 64, 64], P('tp'), may hold values from -0.75 to 0.75
- base_decay_logits: float32 [1024], P('tp'), may hold values from 4 to 11
- extra_log_decay: float32 [3072, 1024], P('fs', 'tp'), may hold values from -0.7 to 0
- mixer_output_matrix: bfloat16 [2048, 1024], P('fs', 'tp'), may hold values from -0.5 to 0.5
- second_norm_scale: float32 [2048], replicated, may hold values from 0.1 to 1.9
- mixer_up_matrix: bfloat16 [2048, 4096], P('fs', 'tp'), may hold values from -0.125 to 0.125
- mixer_down_matrix: bfloat16 [2048, 4096], P('fs', 'tp'), may hold values from -0.09375 to 0.09375
Outputs:
- layer_out: bfloat16 [3072, 2048], P(('fs', 'tp'))
All inputs are finite; a program needn't handle non-finite values.
Results may differ from a plain program's by a relative error of at most 0.022.
Values may be sent and summed in bfloat16 or wider, within the bound.
A program may use at most 64 MiB of HBM per device.

v0:
```python
import jax
import jax.numpy as jnp
from jax import lax
from jax.sharding import PartitionSpec as P

epsilon = 1e-06
decay_rate_scale = 8.0


def rms_scaled(sequence_token_rows, scales):
    widened = sequence_token_rows.astype(jnp.float32)
    mean_square = jnp.mean(widened * widened, axis=-1, keepdims=True)
    return (widened * lax.rsqrt(mean_square + epsilon) * scales).astype(jnp.bfloat16)


def linear_combine(earlier, later):
    return (earlier[0] * later[0], later[0] * earlier[1] + later[1])


def causal_taps(branch, filter_taps_weight):
    tap_count = filter_taps_weight.shape[0]
    positions = branch.shape[0]
    padded = jnp.pad(branch.astype(jnp.float32), ((tap_count - 1, 0), (0, 0)))
    running = jnp.zeros(branch.shape, jnp.float32)
    for offset in range(tap_count):
        running = running + padded[offset : offset + positions] * filter_taps_weight[offset].astype(
            jnp.float32
        )
    return running.astype(jnp.bfloat16)


def block_map(convolved, blocks):
    positions, channels = convolved.shape
    grouped = convolved.reshape(positions, blocks.shape[0], blocks.shape[1])
    mapped = jnp.einsum("sgi,gij->sgj", grouped, blocks, preferred_element_type=jnp.float32)
    return jax.nn.sigmoid(mapped.reshape(positions, channels))


def contract_columns(left, right):
    return lax.dot_general(
        left, right, (((1,), (1,)), ((), ())), preferred_element_type=jnp.float32
    )


def local(
    tokens,
    first_norm_scale,
    recurrent_branch_matrix,
    gelu_gate_matrix,
    filter_taps_weight,
    recurrence_gate_blocks,
    input_gate_blocks,
    base_decay_logits,
    extra_log_decay,
    mixer_output_matrix,
    second_norm_scale,
    mixer_up_matrix,
    mixer_down_matrix,
):
    positions = tokens.shape[0]
    own_count = positions // lax.axis_size("tp")
    normed = rms_scaled(tokens, first_norm_scale)
    branch_sum = jnp.dot(
        normed,
        lax.all_gather(recurrent_branch_matrix, "fs", axis=0, tiled=True),
        preferred_element_type=jnp.float32,
    )
    gate_sum = jnp.dot(
        normed,
        lax.all_gather(gelu_gate_matrix, "fs", axis=0, tiled=True),
        preferred_element_type=jnp.float32,
    )
    branch = branch_sum.astype(jnp.bfloat16)
    gate_branch = gate_sum.astype(jnp.bfloat16)
    out_full = lax.all_gather(mixer_output_matrix, "fs", axis=0, tiled=True)
    convolved = causal_taps(branch, filter_taps_weight)
    recurrence_gate_value = block_map(convolved, recurrence_gate_blocks)
    admission = block_map(convolved, input_gate_blocks)
    log_keep_factor = (
        decay_rate_scale * recurrence_gate_value * jax.nn.log_sigmoid(base_decay_logits)
        + extra_log_decay
    )
    retain = jnp.exp(log_keep_factor)
    driven = jnp.sqrt(-jnp.expm1(2.0 * log_keep_factor)) * (
        admission * convolved.astype(jnp.float32)
    )
    memory = lax.associative_scan(linear_combine, (retain, driven), axis=0)[1]
    recurrent = (memory * jax.nn.gelu(gate_branch.astype(jnp.float32))).astype(jnp.bfloat16)
    up_full = lax.all_gather(mixer_up_matrix, "fs", axis=0, tiled=True)
    whole_sum = lax.psum(contract_columns(recurrent, out_full).astype(jnp.bfloat16), "tp").astype(
        jnp.float32
    )
    residual_all = (tokens.astype(jnp.float32) + whole_sum).astype(jnp.bfloat16)
    raised = jnp.dot(
        rms_scaled(residual_all, second_norm_scale), up_full, preferred_element_type=jnp.float32
    )
    hidden = jnp.square(jax.nn.relu(raised)).astype(jnp.bfloat16)
    residual = lax.dynamic_slice_in_dim(
        residual_all, lax.axis_index("tp") * own_count, own_count, 0
    )
    down_full = lax.all_gather(mixer_down_matrix, "fs", axis=0, tiled=True)
    channel_sum = lax.psum_scatter(
        contract_columns(hidden, down_full).astype(jnp.bfloat16),
        "tp",
        scatter_dimension=0,
        tiled=True,
    ).astype(jnp.float32)
    return (residual.astype(jnp.float32) + channel_sum).astype(jnp.bfloat16)


def solution(mesh):
    in_specs = (
        P("fs", None),
        P(),
        P("fs", "tp"),
        P("fs", "tp"),
        P(None, "tp"),
        P("tp", None, None),
        P("tp", None, None),
        P("tp"),
        P("fs", "tp"),
        P("fs", "tp"),
        P(),
        P("fs", "tp"),
        P("fs", "tp"),
    )
    out_specs = P(("fs", "tp"), None)
    return jax.shard_map(local, mesh=mesh, in_specs=in_specs, out_specs=out_specs, check_vma=False)
```

profile of v0, /device:TPU:0, one launch (start us, length us, event | category | flops | bytes accessed | tf_op | source)
XLA Modules:
  0.0 372.9 jit_solution(10167174261476025850)
XLA Ops:
  6.5 0.7 all-gather.6.cloned.1.call-update
  7.3 0.7 all-gather.10.cloned.1.call-update
  8.1 0.7 all-gather.8.cloned.1.call-update
  8.8 0.8 slice_convert_fusion.3
  9.6 1.8 fusion.3
  11.4 0.7 fusion.59
  12.1 40.4 %all-gather.6.cloned.1.call-done = bf16[2048,256]{1,0:T(8,128)(2,1)} async-done(((bf16[256,256]{1,0:T(8,128)(2,1)}), bf16[2048,256]{1,0:T(8,128)(2,1)}) %all-gather.6.cloned.1.call-update) | async-done | bytes 1048592 | tf_op jit(solution)/shard_map/all_gather | solution.py:65
  52.5 2.3 fusion.20
  54.9 0.2 add_convert_fusion.1
  55.0 0.2 copy.20
  55.2 0.3 fusion.18
  55.5 0.2 copy.22
  55.7 0.3 fusion.15
  56.0 0.2 copy.24
  56.2 0.5 fusion.49
  56.8 0.1 slice.222
  57.0 0.1 slice.220
  57.1 0.1 slice.224
  58.3 0.3 slice.278
  58.6 0.3 slice.219
  59.8 33.8 %all-gather.10.cloned.1.call-done = bf16[2048,256]{1,0:T(8,128)(2,1)} async-done(((bf16[256,256]{1,0:T(8,128)(2,1)}), bf16[2048,256]{1,0:T(8,128)(2,1)}) %all-gather.10.cloned.1.call-update) | async-done | bytes 1048592 | tf_op jit(solution)/shard_map/all_gather | solution.py:75
  93.6 41.2 %all-gather.8.cloned.1.call-done = bf16[2048,256]{1,0:T(8,128)(2,1)} async-done(((bf16[256,256]{1,0:T(8,128)(2,1)}), bf16[2048,256]{1,0:T(8,128)(2,1)}) %all-gather.8.cloned.1.call-update) | async-done | bytes 1048592 | tf_op jit(solution)/shard_map/all_gather | solution.py:70
  134.8 4.6 %convolution_convert_fusion.1 = bf16[384,2048]{1,0:T(8,128)(2,1)} fusion(bf16[2048,256]{1,0:T(8,128)(2,1)} %all-gather.10.cloned.1.call-done, bf16[2048,256]{1,0:T(8,128)(2,1)} %all-gather.8.cloned.1.call-done, bf16[384,2048]{1,0:T(8,128)(2,1)S(1)} %copy-done.1, f32[2048]{0:T(1024)S(1)} %copy-done.4, f32[384]{0:T(512)S(1)} %add_rsqrt_fusion.1, ...), kind=kOutput, calls=%fused_computation.13 | convolution fusion | flops 810516480 | bytes 6039040 | tf_op jit(solution)/shard_map/dot_general | solution.py:40
  139.5 0.5 all-gather.12.cloned.1.call-update
  140.1 0.5 all-gather.14.cloned.1.call-update
  140.7 40.5 %all-reduce.19.cloned.1.call-done = bf16[384,2048]{1,0:T(8,128)(2,1)} async-done(((bf16[384,2048]{1,0:T(8,128)(2,1)}), bf16[384,2048]{1,0:T(8,128)(2,1)}) %all-reduce.19.cloned.1.call-update) | async-done | bytes 1572880 | tf_op jit(solution)/shard_map/psum | solution.py:90
  181.2 2.1 fusion
  183.3 72.7 %all-gather.12.cloned.1.call-done = bf16[2048,1024]{1,0:T(8,128)(2,1)} async-done(((bf16[256,1024]{1,0:T(8,128)(2,1)}), bf16[2048,1024]{1,0:T(8,128)(2,1)}) %all-gather.12.cloned.1.call-update) | async-done | bytes 4194320 | tf_op jit(solution)/shard_map/all_gather | solution.py:89
  256.0 73.3 %all-gather.14.cloned.1.call-done = bf16[2048,1024]{1,0:T(8,128)(2,1)} async-done(((bf16[256,1024]{1,0:T(8,128)(2,1)}), bf16[2048,1024]{1,0:T(8,128)(2,1)}) %all-gather.14.cloned.1.call-update) | async-done | bytes 4194320 | tf_op jit(solution)/shard_map/all_gather | solution.py:101
  329.4 8.1 %convolution_convert_fusion = bf16[384,2048]{1,0:T(8,128)(2,1)} fusion(bf16[2048,1024]{1,0:T(8,128)(2,1)} %all-gather.14.cloned.1.call-done, bf16[2048,1024]{1,0:T(8,128)(2,1)} %all-gather.12.cloned.1.call-done, bf16[384,2048]{1,0:T(8,128)(2,1)S(1)} %get-tuple-element.6, f32[2048]{0:T(1024)S(1)} %copy-done.5, f32[384]{0:T(512)S(1)} %add_rsqrt_fusion), kind=kOutput, calls=%fused_computation.12 | convolution fusion | flops 3226337280 | bytes 11544064 | tf_op jit(solution)/shard_map/dot_general | solution.py:40
  337.6 26.7 %reduce-scatter.2.cloned.1.call-done = bf16[96,2048]{1,0:T(8,128)(2,1)} async-done(((bf16[384,2048]{1,0:T(8,128)(2,1)}), bf16[96,2048]{1,0:T(8,128)(2,1)}) %reduce-scatter.2.cloned.1.call-update) | async-done | bytes 393232 | tf_op jit(solution)/shard_map/reduce_scatter | solution.py:102
  364.2 1.8 add_convert_fusion
  (112 shorter events, 2.0 us)
Async XLA Ops:
  6.5 48.7 %copy-start = (bf16[4,64,64]{2,1,0:T(8,128)(2,1)S(1)}, bf16[4,64,64]{2,1,0:T(8,128)(2,1)}, u32[]{:S(2)}) copy-start(bf16[4,64,64]{2,1,0:T(8,128)(2,1)} %param.18) | copy-start | bytes 98308
  6.5 46.0 %all-gather.6.cloned.1.call-start = ((), (), s32[]{:S(2)}) async-start(), calls=%async_computation.1 | async-start | bytes 1179648 | tf_op jit(solution)/shard_map/all_gather | solution.py:65
  7.3 86.4 %all-gather.10.cloned.1.call-start = ((), (), s32[]{:S(2)}) async-start(), calls=%async_computation.3 | async-start | bytes 1179648 | tf_op jit(solution)/shard_map/all_gather | solution.py:75
  8.0 126.8 %all-gather.8.cloned.1.call-start = ((), (), s32[]{:S(2)}) async-start(), calls=%async_computation.2 | async-start | bytes 1179648 | tf_op jit(solution)/shard_map/all_gather | solution.py:70
  8.7 172.4 %all-reduce.19.cloned.1.call-start = ((), (), s32[]{:S(2)}) async-start(), calls=%async_computation.4 | async-start | bytes 3145728 | tf_op jit(solution)/shard_map/psum | solution.py:90
  12.1 43.6 %copy-start.3 = (bf16[4,64,64]{2,1,0:T(8,128)(2,1)S(1)}, bf16[4,64,64]{2,1,0:T(8,128)(2,1)}, u32[]{:S(2)}) copy-start(bf16[4,64,64]{2,1,0:T(8,128)(2,1)} %param.19) | copy-start | bytes 98308
  54.8 1.4 copy-start.2
  59.1 75.7 %copy-start.1 = (bf16[384,2048]{1,0:T(8,128)(2,1)S(1)}, bf16[384,2048]{1,0:T(8,128)(2,1)}, u32[]{:S(2)}) copy-start(bf16[384,2048]{1,0:T(8,128)(2,1)} %param.13) | copy-start | bytes 4718596
  59.1 75.7 %copy-start.4 = (f32[2048]{0:T(1024)S(1)}, f32[2048]{0:T(1024)}, u32[]{:S(2)}) copy-start(f32[2048]{0:T(1024)} %param.14) | copy-start | bytes 24580
  139.5 189.9 %copy-start.5 = (f32[2048]{0:T(1024)S(1)}, f32[2048]{0:T(1024)}, u32[]{:S(2)}) copy-start(f32[2048]{0:T(1024)} %param.23) | copy-start | bytes 24580
  139.5 116.6 %all-gather.12.cloned.1.call-start = ((), (), s32[]{:S(2)}) async-start(), calls=%async_computation.5 | async-start | bytes 4718592 | tf_op jit(solution)/shard_map/all_gather | solution.py:89
  140.1 189.3 %all-gather.14.cloned.1.call-start = ((), (), s32[]{:S(2)}) async-start(), calls=%async_computation.6 | async-start | bytes 4718592 | tf_op jit(solution)/shard_map/all_gather | solution.py:101
  140.6 223.6 %reduce-scatter.2.cloned.1.call-start = ((), (), s32[]{:S(2)}) async-start(), calls=%async_computation.7 | async-start | bytes 1966080 | tf_op jit(solution)/shard_map/reduce_scatter | solution.py:102
Sparse Core Ops, SparseCore 0:
  9.5 42.9 all-gather.5
  54.6 38.9 all-gather.9
  95.8 38.9 all-gather.7
  139.6 41.5 all-reduce.18
  183.2 72.8 all-gather.11
  258.0 71.3 all-gather.13
  337.7 26.5 reduce-scatter.1
where the time goes:
time: 373 us
  waiting for transfers between devices  332 us (89%)
  matrix products  15.7 us (4%)
  between operations  14.1 us (4%)
  other arithmetic  8.42 us (2%)
    all_gather x1, waiting for transfers between devices, local(): down_full = lax.all_gather(mixer_down_matrix, 'fs', axis=0, tiled=True)  73.3 us
    all_gather x1, waiting for transfers between devices, local(): up_full = lax.all_gather(mixer_up_matrix, 'fs', axis=0, tiled=True)  72.7 us
    all_gather x1, waiting for transfers between devices, local(): lax.all_gather(gelu_gate_matrix, 'fs', axis=0, tiled=True)  41.2 us
    psum x1, waiting for transfers between devices, local(): lax.psum(contract_columns(recurrent, out_full).astype(jnp.bfloat16), 'tp')  40.5 us
    all_gather x1, waiting for transfers between devices, local(): lax.all_gather(recurrent_branch_matrix, 'fs', axis=0, tiled=True)  40.4 us
    all_gather x1, waiting for transfers between devices, local(): out_full = lax.all_gather(mixer_output_matrix, 'fs', axis=0, tiled=True)  33.8 us
    reduce_scatter x1, waiting for transfers between devices, local(): lax.psum_scatter(contract_columns(hidden, down_full).astype(jnp.bfloat16)...  26.7 us
    dot_general x2, matrix products, contract_columns(): lax.dot_general(left, right, (((1,), (1,)), ((), ())), preferred_element_...  12.8 us
  transfers between devices with their start and end apart: 7, of which 7 were waited for; matrix products, arithmetic and copies ran while one was open for 3% of the time, Pallas kernels for 0%

commit v1 on v0

--- a/solution.py
+++ b/solution.py
@@ -1,6 +1,10 @@
+import functools
+
 import jax
 import jax.numpy as jnp
 from jax import lax
+from jax.experimental import pallas as pl
+from jax.experimental.pallas import tpu as pltpu
 from jax.sharding import PartitionSpec as P
 
 epsilon = 1e-06
@@ -108,6 +112,410 @@
     return (residual.astype(jnp.float32) + channel_sum).astype(jnp.bfloat16)
 
 
+MESH = pl.DeviceIdType.MESH
+Y_SIZE = 2
+GROUPS = 4
+
+
+def fits(mesh):
+    n_fs, n_tp = mesh.shape["fs"], mesh.shape["tp"]
+    return n_tp == 2 * Y_SIZE and n_fs == 4 * Y_SIZE
+
+
+def shifted_down(values, by, fill):
+    if by % 8 == 0:
+        top = jnp.full((by, values.shape[1]), fill, values.dtype)
+        return jnp.concatenate([top, values[: values.shape[0] - by]], axis=0)
+    rows = lax.broadcasted_iota(jnp.int32, values.shape, 0)
+    return jnp.where(rows < by, fill, pltpu.roll(values, by, 0))
+
+
+def one_minus_exp(exponent):
+    series = 1.0
+    for order in range(8, 1, -1):
+        series = 1.0 + exponent * (1.0 / order) * series
+    return jnp.where(exponent > -0.35, -exponent * series, 1.0 - jnp.exp(exponent))
+
+
+def fused(
+    nz,
+    tok, scale1, wb, wg, taps, rblk, iblk, logits, extra, wo, scale2, wu, wd,
+    out,
+    normed, fb, fg, fo, fu, fd, rdiag, idiag,
+    part, pair1, give2, got2, res, mid, hidden,
+    part_f, pair_f, give_f, got_f,
+    send_sem, recv_sem, a_send, a_recv, b_send, b_recv,
+):
+    f = lax.axis_index("fs")
+    t = lax.axis_index("tp")
+    z, y = f // Y_SIZE, f % Y_SIZE
+    x, c = t // 2, t % 2
+    last = nz - 1
+    ymate = z * Y_SIZE + (1 - y)
+    xmate = (1 - x) * 2 + c
+    cmate = x * 2 + (1 - c)
+    rows, width = tok.shape
+    own_rows = out.shape[0]
+    depth = wb.shape[0]
+    half = depth // 2
+
+    barrier = pltpu.get_barrier_semaphore()
+    zup = lax.rem(z + 1, nz) * Y_SIZE + y
+    zdown = lax.rem(z + nz - 1, nz) * Y_SIZE + y
+    for other in (zup, zdown, ymate):
+        pl.semaphore_signal(barrier, inc=1, device_id={"fs": other, "tp": t}, device_id_type=MESH)
+    for other in (xmate, cmate):
+        pl.semaphore_signal(barrier, inc=1, device_id={"fs": f, "tp": other}, device_id_type=MESH)
+    pl.semaphore_wait(barrier, 5)
+
+    pieces = (
+        (wb, fb, 0, depth, False),
+        (wg, fg, 0, depth, False),
+        (wo, fo, 0, depth, False),
+        (wu, fu, 0, half, False),
+        (wu, fu, half, half, True),
+        (wd, fd, 0, half, False),
+        (wd, fd, half, half, True),
+    )
+    sent = []
+
+    def slot(g, shard):
+        _, full, first, count, _ = pieces[g]
+        return full.at[pl.ds(pl.multiple_of(shard * depth + first, half), count), :]
+
+    def give(g, shard, way, pred, source=None):
+        target = (zup, zdown, ymate)[way]
+        here = slot(g, shard)
+        copy = pltpu.make_async_remote_copy(
+            src_ref=here if source is None else source,
+            dst_ref=here,
+            send_sem=send_sem.at[g, shard, way],
+            recv_sem=recv_sem.at[g, shard],
+            device_id={"fs": target, "tp": t},
+            device_id_type=MESH,
+        )
+        if pred is None:
+            copy.start()
+            sent.append((None, copy))
+        else:
+            pl.when(pred)(copy.start)
+            sent.append((pred, copy))
+
+    def take(g, shard):
+        here = slot(g, shard)
+        pltpu.make_async_remote_copy(
+            src_ref=here,
+            dst_ref=here,
+            send_sem=send_sem.at[g, shard, 0],
+            recv_sem=recv_sem.at[g, shard],
+            device_id={"fs": ymate, "tp": t},
+            device_id_type=MESH,
+        ).wait_recv()
+
+    def own(g):
+        w, _, first, count, _ = pieces[g]
+        source = w.at[pl.ds(first, count), :]
+        give(g, f, 0, z < last, source)
+        give(g, f, 1, z > 0, source)
+        give(g, f, 2, None, source)
+
+    def wave(g, d):
+        along = pieces[g][4]
+        for way in (0, 1):
+            edge = 0 if way == 0 else last
+            zs = z - d if way == 0 else z + d
+            exists = zs >= 0 if way == 0 else zs <= last
+            onward = z < last if way == 0 else z > 0
+            if d > 0:
+                shard = zs * Y_SIZE + y
+                pl.when(exists)(functools.partial(take, g, shard))
+                give(g, shard, way, exists & onward)
+                if along:
+                    give(g, shard, 2, exists & (zs != 0) & (zs != last))
+                else:
+                    give(g, shard, 2, exists)
+            if along:
+                outer = zs == edge
+                shard = edge * Y_SIZE + (1 - y)
+                pl.when(outer)(functools.partial(take, g, shard))
+                give(g, shard, way, outer & onward)
+
+    def take_across(g):
+        for zs in range(nz):
+            if not (pieces[g][4] and zs in (0, last)):
+                take(g, zs * Y_SIZE + (1 - y))
+
+    def tp_copy(source, target, other, index, send, recv):
+        return pltpu.make_async_remote_copy(
+            src_ref=source,
+            dst_ref=target,
+            send_sem=send.at[index],
+            recv_sem=recv.at[index],
+            device_id={"fs": f, "tp": other},
+            device_id_type=MESH,
+        )
+
+    own(0)
+    own(1)
+    own(2)
+    own(3)
+
+    place = pl.ds(pl.multiple_of(f * depth, depth), depth)
+    fb[place, :] = wb[...]
+    fg[place, :] = wg[...]
+    fo[place, :] = wo[...]
+    fu[place, :] = wu[...]
+    fd[place, :] = wd[...]
+    block = rblk.shape[1]
+    for blocks, diag in ((rblk, rdiag), (iblk, idiag)):
+        diag[...] = jnp.zeros_like(diag)
+        for b in range(rblk.shape[0]):
+            diag[b * block : (b + 1) * block, b * block : (b + 1) * block] = blocks[b]
+
+    def norm_rows(i, carry):
+        at = pl.ds(pl.multiple_of(i * 32, 32), 32)
+        normed[at, :] = rms_scaled(tok[at, :], scale1[...])
+        return carry
+
+    lax.fori_loop(0, rows // 32, norm_rows, 0)
+
+    for d in range(1, nz):
+        wave(0, d)
+        wave(1, d)
+    own(4)
+    wave(2, 1)
+    take_across(0)
+    take_across(1)
+
+    branch = jnp.dot(normed[...], fb[...], preferred_element_type=jnp.float32)
+    branch = branch.astype(jnp.bfloat16).astype(jnp.float32)
+    tap_count = taps.shape[0]
+    running = branch * taps[tap_count - 1 : tap_count, :].astype(jnp.float32)
+    for offset in range(tap_count - 1):
+        by = tap_count - 1 - offset
+        running = running + shifted_down(branch, by, 0.0) * taps[offset : offset + 1, :].astype(
+            jnp.float32
+        )
+    convolved = running.astype(jnp.bfloat16)
+    rate = jax.nn.sigmoid(jnp.dot(convolved, rdiag[...], preferred_element_type=jnp.float32))
+    admission = jax.nn.sigmoid(jnp.dot(convolved, idiag[...], preferred_element_type=jnp.float32))
+    base = -jnp.log1p(jnp.exp(-logits[...]))
+    log_keep = decay_rate_scale * rate * base + extra[...]
+    keep = jnp.exp(log_keep)
+    memory = jnp.sqrt(one_minus_exp(2.0 * log_keep)) * (admission * convolved.astype(jnp.float32))
+    by = 1
+    while by < rows:
+        memory = keep * shifted_down(memory, by, 0.0) + memory
+        if 2 * by < rows:
+            keep = keep * shifted_down(keep, by, 1.0)
+        by *= 2
+    gate = jnp.dot(normed[...], fg[...], preferred_element_type=jnp.float32)
+    gate = gate.astype(jnp.bfloat16).astype(jnp.float32)
+    recurrent = (memory * jax.nn.gelu(gate)).astype(jnp.bfloat16)
+
+    wave(2, 2)
+    wave(2, 3)
+    wave(3, 1)
+    own(5)
+    take_across(2)
+    for k in range(width // depth):
+        product = contract_columns(recurrent, fo[k * depth : (k + 1) * depth, :])
+        part[:, :, k * depth : (k + 1) * depth] = product.astype(jnp.bfloat16).reshape(
+            part.shape[0], own_rows, depth
+        )
+    first = [
+        tp_copy(part.at[2 * other + (1 - c)], pair1.at[other], cmate, other, a_send, a_recv)
+        for other in range(2)
+    ]
+    for copy in first:
+        copy.start()
+    wave(3, 2)
+    for copy in first:
+        copy.wait_recv()
+    away = part[2 * (1 - x) + c].astype(jnp.float32) + pair1[1 - x].astype(jnp.float32)
+    give2[...] = away.astype(jnp.bfloat16)
+    second = tp_copy(give2, got2, xmate, 2, a_send, a_recv)
+    second.start()
+    own(6)
+    wave(3, 3)
+    wave(4, 0)
+    wave(4, 1)
+    second.wait_recv()
+    own_at = pl.ds(pl.multiple_of(t * own_rows, own_rows), own_rows)
+    mixed = part[t].astype(jnp.float32) + pair1[x].astype(jnp.float32)
+    mixed = mixed + got2[...].astype(jnp.float32)
+    residual = (tok[own_at, :].astype(jnp.float32) + mixed).astype(jnp.bfloat16)
+    res[...] = residual
+    mid[t] = rms_scaled(residual, scale2[...])
+    spread = [
+        tp_copy(mid.at[t], mid.at[t], xmate, 3, a_send, a_recv),
+        tp_copy(mid.at[t], mid.at[t], cmate, 4, a_send, a_recv),
+    ]
+    for copy in spread:
+        copy.start()
+    wave(4, 2)
+    wave(5, 1)
+    tp_copy(mid.at[xmate], mid.at[xmate], xmate, 3, a_send, a_recv).wait_recv()
+    relay = tp_copy(mid.at[xmate], mid.at[xmate], cmate, 5, a_send, a_recv)
+    relay.start()
+    wave(4, 3)
+    wave(5, 2)
+    tp_copy(mid.at[cmate], mid.at[cmate], cmate, 4, a_send, a_recv).wait_recv()
+    diagonal = (1 - x) * 2 + (1 - c)
+    tp_copy(mid.at[diagonal], mid.at[diagonal], cmate, 5, a_send, a_recv).wait_recv()
+    take_across(3)
+    take_across(4)
+
+    tile = 256
+
+    def up_tile(i, carry):
+        at = pl.ds(pl.multiple_of(i * tile, tile), tile)
+        raised = jnp.dot(
+            mid[...].reshape(rows, width), fu[:, at], preferred_element_type=jnp.float32
+        )
+        hidden[:, at] = jnp.square(jnp.maximum(raised, 0.0)).astype(jnp.bfloat16)
+        return carry
+
+    lax.fori_loop(0, fu.shape[1] // tile, up_tile, 0)
+
+    wave(5, 3)
+    for d in range(nz):
+        wave(6, d)
+
+    span = width // GROUPS
+    side = z // (nz // 2)
+    firsts, seconds = [], []
+
+    def finish_first(j):
+        for copy in firsts[j]:
+            copy.wait_recv()
+        away = part_f[j, 2 * (1 - x) + c].astype(jnp.float32) + pair_f[j, 1 - x].astype(jnp.float32)
+        give_f[j] = away.astype(jnp.bfloat16)
+        copy = tp_copy(give_f.at[j], got_f.at[j], xmate, 3 * j + 2, b_send, b_recv)
+        copy.start()
+        seconds.append(copy)
+
+    def columns(j):
+        return pl.ds(pl.multiple_of((j + side * (last - 2 * j)) * span, span), span)
+
+    def finish_second(j):
+        seconds[j].wait_recv()
+        total = part_f[j, t].astype(jnp.float32) + pair_f[j, x].astype(jnp.float32)
+        total = total + got_f[j].astype(jnp.float32)
+        out[:, columns(j)] = (res[:, columns(j)].astype(jnp.float32) + total).astype(jnp.bfloat16)
+
+    for j in range(GROUPS):
+        q = j + side * (last - 2 * j)
+        take(5, q * Y_SIZE + (1 - y))
+        if j not in (0, last):
+            take(6, q * Y_SIZE + (1 - y))
+        product = contract_columns(hidden[...], fd[columns(j), :])
+        part_f[j] = product.astype(jnp.bfloat16).reshape(part.shape[0], own_rows, span)
+        copies = [
+            tp_copy(
+                part_f.at[j, 2 * other + (1 - c)], pair_f.at[j, other], cmate, 3 * j + other,
+                b_send, b_recv,
+            )
+            for other in range(2)
+        ]
+        for copy in copies:
+            copy.start()
+        firsts.append(copies)
+        if j > 0:
+            finish_first(j - 1)
+    finish_first(GROUPS - 1)
+    for j in range(GROUPS):
+        finish_second(j)
+
+    for pred, copy in sent:
+        if pred is None:
+            copy.wait_send()
+        else:
+            pl.when(pred)(copy.wait_send)
+    for copy in first + [second] + spread + [relay] + seconds:
+        copy.wait_send()
+    for copies in firsts:
+        for copy in copies:
+            copy.wait_send()
+
+
+def fused_local(
+    mesh,
+    tokens,
+    first_norm_scale,
+    recurrent_branch_matrix,
+    gelu_gate_matrix,
+    filter_taps_weight,
+    recurrence_gate_blocks,
+    input_gate_blocks,
+    base_decay_logits,
+    extra_log_decay,
+    mixer_output_matrix,
+    second_norm_scale,
+    mixer_up_matrix,
+    mixer_down_matrix,
+):
+    n_fs, n_tp = mesh.shape["fs"], mesh.shape["tp"]
+    rows, width = tokens.shape
+    own_rows = rows // n_tp
+    channels = recurrent_branch_matrix.shape[1]
+    units = mixer_up_matrix.shape[1]
+    span = width // GROUPS
+    low, high = jnp.bfloat16, jnp.float32
+    vmem = pl.BlockSpec(memory_space=pltpu.VMEM)
+    return pl.pallas_call(
+        functools.partial(fused, n_fs // Y_SIZE),
+        out_shape=jax.ShapeDtypeStruct((own_rows, width), low),
+        in_specs=[vmem] * 13,
+        out_specs=vmem,
+        scratch_shapes=[
+            pltpu.VMEM((rows, width), low),
+            pltpu.VMEM((width, channels), low),
+            pltpu.VMEM((width, channels), low),
+            pltpu.VMEM((width, channels), low),
+            pltpu.VMEM((width, units), low),
+            pltpu.VMEM((width, units), low),
+            pltpu.VMEM((channels, channels), low),
+            pltpu.VMEM((channels, channels), low),
+            pltpu.VMEM((n_tp, own_rows, width), low),
+            pltpu.VMEM((2, own_rows, width), low),
+            pltpu.VMEM((own_rows, width), low),
+            pltpu.VMEM((own_rows, width), low),
+            pltpu.VMEM((own_rows, width), low),
+            pltpu.VMEM((n_tp, own_rows, width), low),
+            pltpu.VMEM((rows, units), low),
+            pltpu.VMEM((GROUPS, n_tp, own_rows, span), low),
+            pltpu.VMEM((GROUPS, 2, own_rows, span), low),
+            pltpu.VMEM((GROUPS, own_rows, span), low),
+            pltpu.VMEM((GROUPS, own_rows, span), low),
+            pltpu.SemaphoreType.DMA((7, n_fs, 3)),
+            pltpu.SemaphoreType.DMA((7, n_fs)),
+            pltpu.SemaphoreType.DMA((6,)),
+            pltpu.SemaphoreType.DMA((6,)),
+            pltpu.SemaphoreType.DMA((3 * GROUPS,)),
+            pltpu.SemaphoreType.DMA((3 * GROUPS,)),
+        ],
+        compiler_params=pltpu.CompilerParams(
+            collective_id=0, has_side_effects=True, vmem_limit_bytes=60 * 1024 * 1024
+        ),
+        name="fused_layer",
+    )(
+        tokens,
+        first_norm_scale.reshape(1, width),
+        recurrent_branch_matrix,
+        gelu_gate_matrix,
+        filter_taps_weight,
+        recurrence_gate_blocks,
+        input_gate_blocks,
+        base_decay_logits.reshape(1, channels),
+        extra_log_decay,
+        mixer_output_matrix,
+        second_norm_scale.reshape(1, width),
+        mixer_up_matrix,
+        mixer_down_matrix,
+    )
+
+
 def solution(mesh):
     in_specs = (
         P("fs", None),
@@ -125,4 +533,5 @@
         P("fs", "tp"),
     )
     out_specs = P(("fs", "tp"), None)
-    return jax.shard_map(local, mesh=mesh, in_specs=in_specs, out_specs=out_specs, check_vma=False)
+    body = functools.partial(fused_local, mesh) if fits(mesh) else local
+    return jax.shard_map(body, mesh=mesh, in_specs=in_specs, out_specs=out_specs, check_vma=False)

time: 373 us -> 136 us (0.36)
  waiting for transfers between devices: 332 us -> 0 us
  Pallas kernels: 0 us -> 134 us
  matrix products: 15.7 us -> 0 us
  between operations: 14.1 us -> 0.01 us
  other arithmetic: 8.42 us -> 0 us
    all_gather x5 -> x0, waiting for transfers between devices: 261 us -> none  [the longest x1 73.3 us: local(): down_full = lax.all_gather(mixer_down_matrix, 'fs', axis=0, tiled=True)]
    pallas_call x0 -> x1, Pallas kernels: none -> 134 us  [fused_local(): pl.pallas_call(functools.partial(fused, n_fs // Y_SIZE), out_shape=jax.Sh...]
    psum x1 -> x0, waiting for transfers between devices: 40.5 us -> none  [local(): lax.psum(contract_columns(recurrent, out_full).astype(jnp.bfloat16), 'tp')]
    reduce_scatter x1 -> x0, waiting for transfers between devices: 26.7 us -> none  [local(): lax.psum_scatter(contract_columns(hidden, down_full).astype(jnp.bfloat16)...]
    dot_general x5 -> x0, matrix products: 15.7 us -> none  [the longest x2 12.8 us: contract_columns(): lax.dot_general(left, right, (((1,), (1,)), ((), ())), preferred_element_...]
    reduce_sum x2 -> x0, other arithmetic: 3.94 us -> none  [rms_scaled(): mean_square = jnp.mean(widened * widened, axis=-1, keepdims=True)]
  transfers between devices with their start and end apart: 7 -> 0, of which waited for: 7 -> 0; matrix products, arithmetic and copies ran while one was open for 3% -> 0% of each run, Pallas kernels for 0% -> 0%
where the time goes in v1:
time: 136 us
  Pallas kernels  134 us (99%)
  local copies, waits for them, and re-layouts  1.77 us (1%)
    pallas_call x1, Pallas kernels, fused_local(): pl.pallas_call(functools.partial(fused, n_fs // Y_SIZE), out_shape=jax.Sh...  134 us

profile of v1, /device:TPU:0, one launch (start us, length us, event | category | flops | bytes accessed | tf_op | source)
XLA Modules:
  0.0 136.1 jit_solution(9746117313604478550)
XLA Ops:
  0.0 134.3 %fused_layer.1 = bf16[96,2048]{1,0:T(8,128)(2,1)} custom-call(bf16[384,2048]{1,0:T(8,128)(2,1)} %tok.1, f32[1,2048]{1,0:T(1,128)} %bitcast.3, bf16[256,256]{1,0:T(8,128)(2,1)} %wb.1, bf16[256,256]{1,0:T(8,128)(2,1)} %wg.1, bf16[4,256]{1,0:T(4,128)(2,1)} %taps.1, bf16[4,64,64]{2,1,0:T(8,128)(2,1)} %rblk.1, bf16[4,64,64]{2,1,0:T(8,128)(2,1)} %iblk.1, ...), custom_call_target="tpu_custom_call" | custom-call | tf_op jit(solution)/shard_map/fused_layer/pallas_call | solution.py:466
  134.3 1.8 %copy.15 = bf16[96,2048]{1,0:T(8,128)(2,1)} copy(bf16[96,2048]{1,0:T(8,128)(2,1)} %fused_layer.1) | data formatting | bytes 786432

commit v2 on v1

--- a/solution.py
+++ b/solution.py
@@ -139,12 +139,12 @@
 
 def fused(
     nz,
-    tok, scale1, wb, wg, taps, rblk, iblk, logits, extra, wo, scale2, wu, wd,
+    tok_in, scale1, wb, wg, taps, rblk, iblk, logits, extra_in, wo, scale2, wu, wd,
     out,
     normed, fb, fg, fo, fu, fd, rdiag, idiag,
     part, pair1, give2, got2, res, mid, hidden,
     part_f, pair_f, give_f, got_f,
-    send_sem, recv_sem, a_send, a_recv, b_send, b_recv,
+    send_sem, recv_sem, a_send, a_recv, b_send, b_recv, l_sem, tok, extra,
 ):
     f = lax.axis_index("fs")
     t = lax.axis_index("tp")
@@ -159,6 +159,12 @@
     depth = wb.shape[0]
     half = depth // 2
 
+    early = [
+        pltpu.make_async_copy(tok_in, tok, l_sem.at[5]),
+        pltpu.make_async_copy(extra_in, extra, l_sem.at[6]),
+    ]
+    for copy in early:
+        copy.start()
     barrier = pltpu.get_barrier_semaphore()
     zup = lax.rem(z + 1, nz) * Y_SIZE + y
     zdown = lax.rem(z + nz - 1, nz) * Y_SIZE + y
@@ -171,7 +177,7 @@
     pieces = (
         (wb, fb, 0, depth, False),
         (wg, fg, 0, depth, False),
-        (wo, fo, 0, depth, False),
+        (wo, fo, 0, depth, True),
         (wu, fu, 0, half, False),
         (wu, fu, half, half, True),
         (wd, fd, 0, half, False),
@@ -258,20 +264,23 @@
     own(0)
     own(1)
     own(2)
-    own(3)
 
     place = pl.ds(pl.multiple_of(f * depth, depth), depth)
-    fb[place, :] = wb[...]
-    fg[place, :] = wg[...]
-    fo[place, :] = wo[...]
-    fu[place, :] = wu[...]
-    fd[place, :] = wd[...]
+    stays = [
+        pltpu.make_async_copy(w, full.at[place, :], l_sem.at[i])
+        for i, (w, full) in enumerate(((wb, fb), (wg, fg), (wo, fo), (wu, fu), (wd, fd)))
+    ]
+    for copy in stays:
+        copy.start()
     block = rblk.shape[1]
     for blocks, diag in ((rblk, rdiag), (iblk, idiag)):
         diag[...] = jnp.zeros_like(diag)
         for b in range(rblk.shape[0]):
             diag[b * block : (b + 1) * block, b * block : (b + 1) * block] = blocks[b]
 
+    for copy in early:
+        copy.wait()
+
     def norm_rows(i, carry):
         at = pl.ds(pl.multiple_of(i * 32, 32), 32)
         normed[at, :] = rms_scaled(tok[at, :], scale1[...])
@@ -279,13 +288,23 @@
 
     lax.fori_loop(0, rows // 32, norm_rows, 0)
 
-    for d in range(1, nz):
-        wave(0, d)
-        wave(1, d)
+    wave(0, 1)
+    wave(1, 1)
+    own(3)
+    wave(2, 0)
+    wave(2, 1)
+    wave(0, 2)
+    wave(1, 2)
     own(4)
-    wave(2, 1)
+    wave(3, 1)
+    wave(0, 3)
+    wave(1, 3)
+    wave(2, 2)
+    own(5)
     take_across(0)
     take_across(1)
+    for copy in stays:
+        copy.wait()
 
     branch = jnp.dot(normed[...], fb[...], preferred_element_type=jnp.float32)
     branch = branch.astype(jnp.bfloat16).astype(jnp.float32)
@@ -313,10 +332,9 @@
     gate = gate.astype(jnp.bfloat16).astype(jnp.float32)
     recurrent = (memory * jax.nn.gelu(gate)).astype(jnp.bfloat16)
 
-    wave(2, 2)
     wave(2, 3)
-    wave(3, 1)
-    own(5)
+    wave(3, 2)
+    own(6)
     take_across(2)
     for k in range(width // depth):
         product = contract_columns(recurrent, fo[k * depth : (k + 1) * depth, :])
@@ -329,17 +347,15 @@
     ]
     for copy in first:
         copy.start()
-    wave(3, 2)
+    wave(4, 0)
     for copy in first:
         copy.wait_recv()
     away = part[2 * (1 - x) + c].astype(jnp.float32) + pair1[1 - x].astype(jnp.float32)
     give2[...] = away.astype(jnp.bfloat16)
     second = tp_copy(give2, got2, xmate, 2, a_send, a_recv)
     second.start()
-    own(6)
+    wave(4, 1)
     wave(3, 3)
-    wave(4, 0)
-    wave(4, 1)
     second.wait_recv()
     own_at = pl.ds(pl.multiple_of(t * own_rows, own_rows), own_rows)
     mixed = part[t].astype(jnp.float32) + pair1[x].astype(jnp.float32)
@@ -363,6 +379,8 @@
     tp_copy(mid.at[cmate], mid.at[cmate], cmate, 4, a_send, a_recv).wait_recv()
     diagonal = (1 - x) * 2 + (1 - c)
     tp_copy(mid.at[diagonal], mid.at[diagonal], cmate, 5, a_send, a_recv).wait_recv()
+    wave(6, 0)
+    wave(6, 1)
     take_across(3)
     take_across(4)
 
@@ -378,12 +396,11 @@
 
     lax.fori_loop(0, fu.shape[1] // tile, up_tile, 0)
 
-    wave(5, 3)
-    for d in range(nz):
-        wave(6, d)
-
     span = width // GROUPS
     side = z // (nz // 2)
+    inner = z + side * (last - 2 * z)
+    ranks = [inner, 1 - inner] + list(range(2, nz))
+    order = [rank + side * (last - 2 * rank) for rank in ranks]
     firsts, seconds = [], []
 
     def finish_first(j):
@@ -396,7 +413,7 @@
         seconds.append(copy)
 
     def columns(j):
-        return pl.ds(pl.multiple_of((j + side * (last - 2 * j)) * span, span), span)
+        return pl.ds(pl.multiple_of(order[j] * span, span), span)
 
     def finish_second(j):
         seconds[j].wait_recv()
@@ -405,10 +422,14 @@
         out[:, columns(j)] = (res[:, columns(j)].astype(jnp.float32) + total).astype(jnp.bfloat16)
 
     for j in range(GROUPS):
-        q = j + side * (last - 2 * j)
+        if j == 1:
+            wave(5, 3)
+        if j > 1:
+            wave(6, j)
+        q = order[j]
         take(5, q * Y_SIZE + (1 - y))
-        if j not in (0, last):
-            take(6, q * Y_SIZE + (1 - y))
+        if j != last:
+            pl.when((q != 0) & (q != last))(functools.partial(take, 6, q * Y_SIZE + (1 - y)))
         product = contract_columns(hidden[...], fd[columns(j), :])
         part_f[j] = product.astype(jnp.bfloat16).reshape(part.shape[0], own_rows, span)
         copies = [
@@ -423,9 +444,11 @@
         firsts.append(copies)
         if j > 0:
             finish_first(j - 1)
+        if j > 1:
+            finish_second(j - 2)
     finish_first(GROUPS - 1)
-    for j in range(GROUPS):
-        finish_second(j)
+    finish_second(GROUPS - 2)
+    finish_second(GROUPS - 1)
 
     for pred, copy in sent:
         if pred is None:
@@ -463,10 +486,11 @@
     span = width // GROUPS
     low, high = jnp.bfloat16, jnp.float32
     vmem = pl.BlockSpec(memory_space=pltpu.VMEM)
+    hbm = pl.BlockSpec(memory_space=pl.ANY)
     return pl.pallas_call(
         functools.partial(fused, n_fs // Y_SIZE),
         out_shape=jax.ShapeDtypeStruct((own_rows, width), low),
-        in_specs=[vmem] * 13,
+        in_specs=[hbm, vmem, hbm, hbm] + [vmem] * 4 + [hbm, hbm, vmem, hbm, hbm],
         out_specs=vmem,
         scratch_shapes=[
             pltpu.VMEM((rows, width), low),
@@ -494,6 +518,9 @@
             pltpu.SemaphoreType.DMA((6,)),
             pltpu.SemaphoreType.DMA((3 * GROUPS,)),
             pltpu.SemaphoreType.DMA((3 * GROUPS,)),
+            pltpu.SemaphoreType.DMA((7,)),
+            pltpu.VMEM((rows, width), low),
+            pltpu.VMEM((rows, channels), high),
         ],
         compiler_params=pltpu.CompilerParams(
             collective_id=0, has_side_effects=True, vmem_limit_bytes=60 * 1024 * 1024

time: 136 us -> 132 us (0.971)
  Pallas kernels: 134 us -> 130 us
    pallas_call x1, Pallas kernels: 134 us -> 130 us  [fused_local(): pl.pallas_call(functools.partial(fused, n_fs // Y_SIZE), out_shape=jax.Sh...]
where the time goes in v2:
time: 132 us
  Pallas kernels  130 us (98%)
  local copies, waits for them, and re-layouts  1.77 us (1%)
    pallas_call x1, Pallas kernels, fused_local(): pl.pallas_call(functools.partial(fused, n_fs // Y_SIZE), out_shape=jax.Sh...  130 us

profile of v2, /device:TPU:0, one launch (start us, length us, event | category | flops | bytes accessed | tf_op | source)
XLA Modules:
  0.0 131.8 jit_solution(11497259537563426874)
XLA Ops:
  0.0 130.0 %fused_layer.1 = bf16[96,2048]{1,0:T(8,128)(2,1)} custom-call(bf16[384,2048]{1,0:T(8,128)(2,1)} %tok_in.1, f32[1,2048]{1,0:T(1,128)} %bitcast.3, bf16[256,256]{1,0:T(8,128)(2,1)} %wb.1, bf16[256,256]{1,0:T(8,128)(2,1)} %wg.1, bf16[4,256]{1,0:T(4,128)(2,1)} %taps.1, bf16[4,64,64]{2,1,0:T(8,128)(2,1)} %rblk.1, bf16[4,64,64]{2,1,0:T(8,128)(2,1)} %iblk.1, ...), custom_call_target="tpu_custom_call" | custom-call | tf_op jit(solution)/shard_map/fused_layer/pallas_call | solution.py:490
  130.0 1.8 %copy.15 = bf16[96,2048]{1,0:T(8,128)(2,1)} copy(bf16[96,2048]{1,0:T(8,128)(2,1)} %fused_layer.1) | data formatting | bytes 786432
